TPU v7x, 32 devices: a whole 2x2x4 slice. The times are simulated.
32 devices in a mesh: sp: 8 (over z, y), tp: 4 (over x, core).
Axes of the slice: x: 2, y: 2, z: 4, core: 2. Of those that a mesh axis runs over, the one named last changes fastest.
Arguments:
- block_input: bfloat16 [8192, 2048], P('sp'), may hold values from -6 to 6
- out_grad: bfloat16 [8192, 2048], P('sp'), may hold values from -6 to 6
- w_value: bfloat16 [2048, 1024], P(None, 'tp'), may hold values from -0.125 to 0.125
- w_gate: bfloat16 [2048, 1024], P(None, 'tp'), may hold values from -0.125 to 0.125
- conv_taps: float32 [31, 1024], P(None, 'tp'), may hold values from -4 to 4
- norm_gain: float32 [1024], P('tp'), may hold values from 0.1 to 1.9
- norm_shift: float32 [1024], P('tp'), may hold values from -3 to 3
- w_proj: bfloat16 [1024, 2048], P('tp'), may hold values from -0.1875 to 0.1875
Outputs:
- input_grad: bfloat16 [8192, 2048], P('sp', 'tp')
- value_wgrad: float32 [2048, 1024], P('sp', 'tp')
- gate_wgrad: float32 [2048, 1024], P('sp', 'tp')
- proj_wgrad: float32 [1024, 2048], P('tp', 'sp')
- taps_grad: float32 [31, 1024], P(None, 'tp')
- gain_grad: float32 [1024], P('tp')
- shift_grad: float32 [1024], P('tp')
All inputs are finite; a program needn't handle non-finite values.
Results may differ from a plain program's by a relative error of at most 0.014.
Values may be sent and summed in bfloat16 or wider, within the bound.
A program may use at most 128 MiB of HBM per device.

v0:
```python
import math

import jax
import jax.numpy as jnp
from jax import lax
from jax.sharding import PartitionSpec as P

CH = 1024


EPS = 0.05


def from_behind(block, axis, distance):
    devices = range(lax.axis_size(axis))
    route = [(i - distance, i) for i in devices if i - distance in devices]
    return lax.ppermute(block, axis, route)


def right_product(left, right):
    return lax.dot_general(
        left, right, (((1,), (1,)), ((), ())), preferred_element_type=jnp.float32
    )


def column_product(left, right):
    return lax.dot_general(
        left, right, (((0,), (0,)), ((), ())), preferred_element_type=jnp.float32
    )


def shards(block_input, out_grad, w_value, w_gate, conv_taps, norm_gain, norm_shift, w_proj):
    tok_rows = block_input.shape[0]
    kernel_len = conv_taps.shape[0]
    reach_back = kernel_len - 1
    channels_dev = w_value.shape[1]
    loss_scale = 1.0 / math.sqrt(tok_rows * lax.axis_size("sp"))
    value_proj = jnp.dot(block_input, w_value, preferred_element_type=jnp.float32).astype(
        jnp.bfloat16
    )
    gate_proj = jnp.dot(block_input, w_gate, preferred_element_type=jnp.float32).astype(
        jnp.bfloat16
    )
    gate_sigmoid = jax.nn.sigmoid(gate_proj.astype(jnp.float32))
    value_wide = value_proj.astype(jnp.float32)
    gated_input = (value_wide * gate_sigmoid).astype(jnp.bfloat16)
    earlier = from_behind(gated_input[tok_rows - reach_back :], "sp", 1)
    extended = jnp.concatenate([earlier, gated_input], axis=0).astype(jnp.float32)
    filtered = jnp.zeros((tok_rows, channels_dev), jnp.float32)
    for tap_index in range(kernel_len):
        begin = reach_back - tap_index
        filtered = filtered + conv_taps[tap_index] * extended[begin : begin + tok_rows]
    row_sum, row_square = lax.psum(
        (jnp.sum(filtered, axis=1), jnp.sum(filtered * filtered, axis=1)), "tp"
    )
    row_mean = row_sum / CH
    row_var = row_square / CH - row_mean * row_mean
    row_scale = lax.rsqrt(row_var + EPS)
    normed = (filtered - row_mean[:, None]) * row_scale[:, None]
    activated = normed * norm_gain + norm_shift
    act_sigmoid = jax.nn.sigmoid(activated)
    mixer_out = (activated * act_sigmoid).astype(jnp.bfloat16)
    grad_mixed = right_product(out_grad, w_proj)
    grad_act = grad_mixed * act_sigmoid * (1.0 + activated * (1.0 - act_sigmoid))
    grad_normed = grad_act * norm_gain
    back_sum, back_cross = lax.psum(
        (jnp.sum(grad_normed, axis=1), jnp.sum(grad_normed * normed, axis=1)), "tp"
    )
    grad_filtered = row_scale[:, None] * (
        grad_normed - back_sum[:, None] / CH - normed * (back_cross[:, None] / CH)
    )
    gain_part = jnp.sum(grad_act * normed, axis=0)
    shift_part = jnp.sum(grad_act, axis=0)
    padded_grad = jnp.pad(grad_filtered, ((reach_back, reach_back), (0, 0)))
    grad_extended = jnp.zeros((tok_rows + reach_back, channels_dev), jnp.float32)
    taps_rows = []
    for tap_index in range(kernel_len):
        begin = reach_back - tap_index
        grad_extended = (
            grad_extended
            + conv_taps[tap_index] * padded_grad[tap_index : tap_index + tok_rows + reach_back]
        )
        taps_rows.append(jnp.sum(grad_filtered * extended[begin : begin + tok_rows], axis=0))
    taps_part = jnp.stack(taps_rows, axis=0)
    returned = from_behind(grad_extended[:reach_back], "sp", -1)
    grad_glu = jnp.concatenate(
        [grad_extended[reach_back:tok_rows], grad_extended[tok_rows:] + returned], axis=0
    )
    grad_value = (grad_glu * gate_sigmoid).astype(jnp.bfloat16)
    grad_gate = (grad_glu * value_wide * gate_sigmoid * (1.0 - gate_sigmoid)).astype(jnp.bfloat16)
    grad_both = jnp.concatenate([grad_value, grad_gate], axis=1)
    small_taps, small_gain, small_shift = lax.psum((taps_part, gain_part, shift_part), "sp")
    partial_input = right_product(grad_value, w_value) + right_product(grad_gate, w_gate)
    input_grad = lax.psum_scatter(
        partial_input.astype(jnp.bfloat16), "tp", scatter_dimension=1, tiled=True
    )
    summed = lax.psum_scatter(
        jnp.concatenate(
            [column_product(block_input, grad_both), column_product(out_grad, mixer_out)], axis=1
        ),
        "sp",
        scatter_dimension=0,
        tiled=True,
    )
    weight_sum = summed[:, : 2 * channels_dev]
    proj_sum = summed[:, 2 * channels_dev :]
    value_wgrad = weight_sum[:, :channels_dev] * loss_scale
    gate_wgrad = weight_sum[:, channels_dev:] * loss_scale
    proj_wgrad = (proj_sum * loss_scale).T
    return (
        input_grad,
        value_wgrad,
        gate_wgrad,
        proj_wgrad,
        small_taps * loss_scale,
        small_gain * loss_scale,
        small_shift * loss_scale,
    )


def solution(mesh):
    return jax.shard_map(
        shards,
        mesh=mesh,
        in_specs=(
            P("sp", None),
            P("sp", None),
            P(None, "tp"),
            P(None, "tp"),
            P(None, "tp"),
            P("tp"),
            P("tp"),
            P("tp", None),
        ),
        out_specs=(
            P("sp", "tp"),
            P("sp", "tp"),
            P("sp", "tp"),
            P("tp", "sp"),
            P(None, "tp"),
            P("tp"),
            P("tp"),
        ),
        check_vma=False,
    )
```

profile of v0, /device:TPU:9, one launch (start us, length us, event | category | flops | bytes accessed | tf_op | source)
XLA Modules:
  0.0 238.3 jit_solution(9940296154718128361)
XLA Ops:
  7.2 0.0 copy-start
  7.2 0.0 reduce-scatter.5.cloned.1.call-start
  7.2 0.0 copy-start.12
  7.2 3.9 %convolution_convert_fusion.1 = bf16[1024,256]{1,0:T(8,128)(2,1)S(1)} fusion(bf16[1024,2048]{1,0:T(8,128)(2,1)} %param.8, bf16[2048,256]{1,0:T(8,128)(2,1)} %param.10), kind=kOutput, calls=%fused_computation.14 | convolution fusion | flops 1074003968 | bytes 5767168 | tf_op jit(solution)/shard_map/dot_general | solution.py:38
  11.1 0.0 copy-done
  11.1 0.1 copy-done.12
  11.3 0.0 copy-start.7
  11.3 2.3 fusion.6
  13.5 0.0 copy-done.7
  13.6 3.1 %collective-permute-start = (bf16[30,256]{1,0:T(8,128)(2,1)S(1)}, bf16[30,256]{1,0:T(8,128)(2,1)S(1)}, u32[]{:S(2)}, u32[]{:S(2)}) collective-permute-start(bf16[30,256]{1,0:T(8,128)(2,1)S(1)} %slice.465), channel_id=1, source_target_pairs={{0,4},{4,8},{8,12},{12,16},{16,20},{20,24},{24,28},{1,5},{5,9},{9,... | collective-permute-start | bytes 46088 | tf_op jit(solution)/shard_map/ppermute | solution.py:17
  16.7 0.0 copy-done.9
  16.8 2.2 collective-permute-done
  18.9 0.1 maximum_convert_fusion
  19.1 0.0 copy-start.10
  19.1 0.0 copy-start.14
  19.1 4.7 %multiply_reduce_fusion.33 = (f32[1024]{0:T(1024)S(1)}, f32[1024]{0:T(1024)S(1)}, f32[1024,256]{1,0:T(8,128)S(1)}) fusion(f32[1054,256]{1,0:T(8,128)S(1)} %maximum_convert_fusion, f32[256]{0:T(256)S(1)} %bitcast.138, f32[256]{0:T(256)S(1)} %bitcast.140, f32[256]{0:T(256)S(1)} %bitcast.82, f32[256]{0:T(256)S(1)} %bitcast.84, f32[256]{0:T(256)S(1)} %bitcast.86, ...), kind=kLoop, calls=%fused_computation.63 | loop fusion | flops 16775168 | bytes 33594368 | tf_op jit(solution)/shard_map/reduce_sum | solution.py:54
  23.7 0.0 copy-start.1
  23.7 6.9 %all-reduce.3 = (f32[1024]{0:T(1024)S(1)}, f32[1024]{0:T(1024)S(1)}) all-reduce(f32[1024]{0:T(1024)S(1)} %get-tuple-element.50, f32[1024]{0:T(1024)S(1)} %get-tuple-element.49), channel_id=1, replica_groups=mesh['sp'=8,'tp'=4] {'tp'}, use_global_device_ids=true, to_apply=%region_3.0 | all-reduce | flops 2048 | bytes 16384 | tf_op jit(solution)/shard_map/psum | solution.py:53
  30.7 0.0 copy-done.10
  30.7 0.0 copy-done.14
  30.7 5.2 %multiply_reduce_fusion = (f32[256]{0:T(256)S(1)}, f32[1024]{0:T(1024)S(1)}, f32[1024]{0:T(1024)S(1)}, f32[256]{0:T(256)S(1)}, f32[1024,256]{1,0:T(8,128)}) fusion(f32[1024,256]{1,0:T(8,128)S(1)} %get-tuple-element.59, f32[1024]{0:T(1024)S(1)} %get-tuple-element.97, f32[1024]{0:T(1024)S(1)} %get-tuple-element.96, f32[256]{0:T(256)S(1)} %copy-done.10, ...), kind=kOutput, calls=%fused_computation.24 | convolution fusion | flops 1078720000 | bytes 7360512 | tf_op jit(solution)/shard_map/dot_general | solution.py:21
  35.9 0.0 copy-done.1
  35.9 5.9 %all-reduce.2 = (f32[1024]{0:T(1024)S(1)}, f32[1024]{0:T(1024)S(1)}) all-reduce(f32[1024]{0:T(1024)S(1)} %get-tuple-element.46, f32[1024]{0:T(1024)S(1)} %get-tuple-element.47), channel_id=1, replica_groups=mesh['sp'=8,'tp'=4] {'tp'}, use_global_device_ids=true, to_apply=%region_7.0 | all-reduce | flops 2048 | bytes 16384 | tf_op jit(solution)/shard_map/psum | solution.py:66
  41.8 0.0 copy-start.11
  41.8 4.4 %multiply_reduce_fusion.1 = (f32[256]{0:T(256)S(1)}, f32[256]{0:T(256)S(1)}, f32[256]{0:T(256)S(1)}, f32[256]{0:T(256)S(1)}, f32[256]{0:T(256)S(1)}, /*index=5*/...) fusion(f32[1054,256]{1,0:T(8,128)S(1)} %maximum_convert_fusion,, ...), kind=kLoop, calls=%fused_computation.25 | loop fusion | flops 11267584 | bytes 22055936 | tf_op jit(solution)/shard_map/reduce_sum | solution.py:83
  46.3 0.0 copy-start.2
  46.3 4.9 %multiply_add_fusion = f32[1054,256]{1,0:T(8,128)S(1)} fusion(f32[1024,256]{1,0:T(8,128)S(1)} %get-tuple-element.58, f32[256]{0:T(256)S(1)} %bitcast.139, f32[256]{0:T(256)S(1)} %bitcast.141, f32[256]{0:T(256)S(1)} %bitcast.83, f32[256]{0:T(256)S(1)} %bitcast.85, f32[256]{0:T(256)S(1)} %bitcast.87, f32[256]{0:T(256)S(1)} %bitcast.89, f32[256]{0:T(256)S(1)} %bitcast.91, ...), kind=kLoop, calls=%fused_computation.15 | loop fusion | flops 16459264 | bytes 2159616 | tf_op jit(solution)/shard_map/add | solution.py:80
  51.2 2.3 collective-permute-start.1
  53.5 0.0 copy-done.11
  53.5 0.0 copy-done.2
  53.5 1.5 convolution_bitcast_fusion.1
  55.1 0.0 copy-start.6
  55.1 0.0 copy-start.8
  55.1 0.0 copy-start.13
  55.1 0.1 slice.497
  55.2 0.7 collective-permute-done.1
  55.8 0.4 copy-done.6
  56.3 0.1 copy-done.8
  56.4 0.3 fusion.9
  56.7 0.0 copy-start.3
  56.8 0.0 copy-start.4
  56.8 1.0 copy-done.13
  57.7 2.4 convolution_bitcast_fusion
  60.1 0.0 copy-done.3
  60.1 0.0 copy-done.4
  60.1 3.1 %pad_maximum_fusion = f32[2048,768]{0,1:T(8,128)} fusion(f32[2048,256]{0,1:T(8,128)S(1)} %convolution_bitcast_fusion.1, f32[2048,512]{0,1:T(8,128)S(1)} %convolution_bitcast_fusion), kind=kLoop, calls=%fused_computation.1 | loop fusion | flops 1572864 | bytes 12582912 | tf_op jit(solution)/shard_map/concatenate | solution.py:98
  63.2 0.0 reduce-scatter.5.cloned.1.call-update
  63.3 0.0 reduce-scatter.3.cloned.1.call-start
  63.3 0.0 copy-start.5
  63.3 2.7 %fusion.23 = f32[1024,2048]{1,0:T(8,128)S(1)} fusion(bf16[1024,256]{1,0:T(8,128)(2,1)} %copy-done.3, bf16[2048,256]{1,0:T(8,128)(2,1)} %param.10), kind=kOutput, calls=%fused_computation.88 | convolution fusion | flops 1073741824 | bytes 9961472 | tf_op jit(solution)/shard_map/dot_general | solution.py:21
  66.0 0.0 copy-done.5
  66.1 3.3 %add_convert_fusion = bf16[1024,2048]{1,0:T(8,128)(2,1)} fusion(f32[1024,2048]{1,0:T(8,128)S(1)} %fusion.23, bf16[1024,256]{1,0:T(8,128)(2,1)S(1)} %copy-done.5, bf16[2048,256]{1,0:T(8,128)(2,1)S(1)} %copy-done), kind=kOutput, calls=%fused_computation | convolution fusion | flops 1077936128 | bytes 14155776 | tf_op jit(solution)/shard_map/dot_general | solution.py:21
  69.4 0.0 reduce-scatter.3.cloned.1.call-update
  69.4 1.8 multiply_reduce_fusion.19
  71.2 0.1 stack.127
  71.3 30.5 %all-reduce.1 = (f32[31,256]{1,0:T(8,128)S(1)}, f32[256]{0:T(256)S(1)}, f32[256]{0:T(256)S(1)}) all-reduce(f32[31,256]{1,0:T(8,128)S(1)} %stack.127, f32[256]{0:T(256)S(1)} %get-tuple-element.45, f32[256]{0:T(256)S(1)} %get-tuple-element.48), channel_id=1, replica_groups=mesh['sp'=8,'tp'=4] {'sp'}, use_global_device_ids=true, to_apply=%region_41.42 | all-reduce | flops 8448 | bytes 67584 | tf_op jit(solution)/shard_map/psum | solution.py:92
  101.8 0.6 broadcast_multiply_fusion.5
  102.3 0.6 broadcast_multiply_fusion.4
  102.9 0.6 broadcast_multiply_fusion
  103.5 80.4 %reduce-scatter.5.cloned.1.call-done = f32[256,768]{0,1:T(8,128)} async-done(((f32[2048,768]{0,1:T(8,128)}), f32[256,768]{0,1:T(8,128)}) %reduce-scatter.5.cloned.1.call-update) | async-done | bytes 786448 | tf_op jit(solution)/shard_map/reduce_scatter | solution.py:97
  183.9 1.9 fusion.18
  185.8 0.8 copy.16
  186.7 0.8 copy.15
  187.5 44.0 %reduce-scatter.3.cloned.1.call-done = bf16[1024,512]{1,0:T(8,128)(2,1)} async-done(((bf16[1024,2048]{1,0:T(8,128)(2,1)}), bf16[1024,512]{1,0:T(8,128)(2,1)}) %reduce-scatter.3.cloned.1.call-update) | async-done | bytes 1048592 | tf_op jit(solution)/shard_map/reduce_scatter | solution.py:94
  (8 shorter events, 0.1 us)
Async XLA Ops:
  7.2 4.0 %copy-start = (bf16[2048,256]{1,0:T(8,128)(2,1)S(1)}, bf16[2048,256]{1,0:T(8,128)(2,1)}, u32[]{:S(2)}) copy-start(bf16[2048,256]{1,0:T(8,128)(2,1)} %param.11) | copy-start | bytes 3145732
  7.2 176.8 %reduce-scatter.5.cloned.1.call-start = ((), (), s32[]{:S(2)}) async-start(), calls=%async_computation.3 | async-start | bytes 7077888 | tf_op jit(solution)/shard_map/reduce_scatter | solution.py:97
  7.2 4.0 %copy-start.12 = (bf16[1024,2048]{1,0:T(8,128)(2,1)S(1)}, bf16[1024,2048]{1,0:T(8,128)(2,1)}, u32[]{:S(2)}) copy-start(bf16[1024,2048]{1,0:T(8,128)(2,1)} %param.8) | copy-start | bytes 12582916
  11.3 2.3 copy-start.7
  11.3 5.4 %copy-start.9 = (f32[31,256]{1,0:T(8,128)S(1)}, f32[31,256]{1,0:T(8,128)}, u32[]{:S(2)}) copy-start(f32[31,256]{1,0:T(8,128)} %param.12) | copy-start | bytes 95236
  13.6 5.4 %collective-permute-start = (bf16[30,256]{1,0:T(8,128)(2,1)S(1)}, bf16[30,256]{1,0:T(8,128)(2,1)S(1)}, u32[]{:S(2)}, u32[]{:S(2)}) collective-permute-start(bf16[30,256]{1,0:T(8,128)(2,1)S(1)} %slice.465), channel_id=1, source_target_pairs={{0,4},{4,8},{8,12},{12,16},{16,20},{20,24},{24,28},{1,5},{5,9},{9,... | collective-permute-start | bytes 46088 | tf_op jit(solution)/shard_map/ppermute | solution.py:17
  19.1 11.6 %copy-start.10 = (f32[256]{0:T(256)S(1)}, f32[256]{0:T(256)}, u32[]{:S(2)}) copy-start(f32[256]{0:T(256)} %param.13) | copy-start | bytes 3076
  19.1 11.6 %copy-start.14 = (f32[256]{0:T(256)S(1)}, f32[256]{0:T(256)}, u32[]{:S(2)}) copy-start(f32[256]{0:T(256)} %param.14) | copy-start | bytes 3076
  23.7 12.2 %copy-start.1 = (f32[1024,256]{1,0:T(8,128)}, f32[1024,256]{1,0:T(8,128)S(1)}, u32[]{:S(2)}) copy-start(f32[1024,256]{1,0:T(8,128)S(1)} %get-tuple-element.59) | copy-start | bytes 3145732
  41.8 11.7 %copy-start.11 = (bf16[1024,2048]{1,0:T(8,128)(2,1)S(1)}, bf16[1024,2048]{1,0:T(8,128)(2,1)}, u32[]{:S(2)}) copy-start(bf16[1024,2048]{1,0:T(8,128)(2,1)} %param.9) | copy-start | bytes 12582916
  46.3 7.2 %copy-start.2 = (f32[1024,256]{1,0:T(8,128)S(1)}, f32[1024,256]{1,0:T(8,128)}, u32[]{:S(2)}) copy-start(f32[1024,256]{1,0:T(8,128)} %copy-done.1) | copy-start | bytes 3145732
  51.2 4.7 %collective-permute-start.1 = (f32[30,256]{1,0:T(8,128)S(1)}, f32[30,256]{1,0:T(8,128)S(1)}, u32[]{:S(2)}, u32[]{:S(2)}) collective-permute-start(f32[30,256]{1,0:T(8,128)S(1)} %slice.499), channel_id=1, source_target_pairs={{4,0},{8,4},{12,8},{16,12},{20,16},{24,20},{28,24},{5,1},{9,5},{13... | collective-permute-start | bytes 92168 | tf_op jit(solution)/shard_map/ppermute | solution.py:17
  55.1 1.2 copy-start.6
  55.1 1.3 copy-start.8
  55.1 2.7 %copy-start.13 = (bf16[1024,2048]{1,0:T(8,128)(2,1)S(1)}, bf16[1024,2048]{1,0:T(8,128)(2,1)}, u32[]{:S(2)}) copy-start(bf16[1024,2048]{1,0:T(8,128)(2,1)} %param.8) | copy-start | bytes 12582916
  56.7 3.4 %copy-start.3 = (bf16[1024,256]{1,0:T(8,128)(2,1)}, bf16[1024,256]{1,0:T(8,128)(2,1)S(1)}, u32[]{:S(2)}) copy-start(bf16[1024,256]{1,0:T(8,128)(2,1)S(1)} %get-tuple-element.61) | copy-start | bytes 1572868
  56.8 3.4 %copy-start.4 = (bf16[1024,256]{1,0:T(8,128)(2,1)}, bf16[1024,256]{1,0:T(8,128)(2,1)S(1)}, u32[]{:S(2)}) copy-start(bf16[1024,256]{1,0:T(8,128)(2,1)S(1)} %get-tuple-element.60) | copy-start | bytes 1572868
  63.3 168.2 %reduce-scatter.3.cloned.1.call-start = ((), (), s32[]{:S(2)}) async-start(), calls=%async_computation.2 | async-start | bytes 5242880 | tf_op jit(solution)/shard_map/reduce_scatter | solution.py:94
  63.3 2.7 %copy-start.5 = (bf16[1024,256]{1,0:T(8,128)(2,1)S(1)}, bf16[1024,256]{1,0:T(8,128)(2,1)}, u32[]{:S(2)}) copy-start(bf16[1024,256]{1,0:T(8,128)(2,1)} %copy-done.4) | copy-start | bytes 1572868
Sparse Core Ops, SparseCore 0:
  63.4 120.5 reduce-scatter.4
  187.0 44.3 reduce-scatter.2
where the time goes:
time: 240 us; the launch traced here: 238 us
  waiting for transfers between devices  127 us (53%)
  blocking collectives  43.3 us (18%)
  other arithmetic  22.9 us (10%)
  matrix products  21.3 us (9%)
  between operations  14.4 us (6%)
  starting transfers between devices  5.55 us (2%)
  local copies, waits for them, and re-layouts  3.64 us (2%)
    reduce_scatter x1, waiting for transfers between devices, shards(): lax.psum_scatter(jnp.concatenate([column_product(block_input, grad_both),...  80.4 us
    reduce_scatter x1, waiting for transfers between devices, shards(): lax.psum_scatter(partial_input.astype(jnp.bfloat16), 'tp', scatter_dimens...  44 us
    psum x1, blocking collectives, shards(): lax.psum((taps_part, gain_part, shift_part), 'sp')  30.5 us
    dot_general x3, matrix products, right_product(): lax.dot_general(left, right, (((1,), (1,)), ((), ())), preferred_element_...  11.3 us
    psum x1, blocking collectives, shards(): lax.psum((jnp.sum(filtered, axis=1), jnp.sum(filtered * filtered, axis=1)...  6.93 us
    reduce_sum x2, other arithmetic, shards(): jnp.sum(grad_filtered * extended[begin:begin + tok_rows], axis=0)  6.2 us
    psum x1, blocking collectives, shards(): lax.psum((jnp.sum(grad_normed, axis=1), jnp.sum(grad_normed * normed, axi...  5.86 us
    ppermute x2, starting transfers between devices, from_behind(): return lax.ppermute(block, axis, route)  5.47 us
  transfers between devices with their start and end apart: 4, of which 4 were waited for; matrix products, arithmetic and copies ran while one was open for 6% of the time, Pallas kernels for 0%

commit v1 on v0

--- a/solution.py
+++ b/solution.py
@@ -1,8 +1,11 @@
+import functools
 import math
 
 import jax
 import jax.numpy as jnp
 from jax import lax
+from jax.experimental import pallas as pl
+from jax.experimental.pallas import tpu as pltpu
 from jax.sharding import PartitionSpec as P
 
 CH = 1024
@@ -27,6 +30,226 @@
     return lax.dot_general(
         left, right, (((0,), (0,)), ((), ())), preferred_element_type=jnp.float32
     )
+
+
+MESH = pl.DeviceIdType.MESH
+
+
+def tail_kernel(
+    n, n_tp, loss_scale,
+    bi_hbm, og_hbm, wv_hbm, wg_hbm, gb_ref, mo_ref, small_ref,
+    ig_ref, ws_ref, ps_ref, sm_ref,
+    bi, og, wv, wg,
+    gs, gr, gs2, gq, pm, pr, ps2, pq,
+    xs, xr, ys, yr, acc, small_pair, small_in, small_all,
+    load_sem,
+    gs_send, gs_recv, gq_send, gq_recv, pr_send, pr_recv, pq_send, pq_recv,
+    x_send, x_recv, y_send, y_recv, s_send, s_recv, sa_send, sa_recv,
+):
+    me, t = lax.axis_index("sp"), lax.axis_index("tp")
+    outer, inner = me // 2, me % 2
+    h = n // 2
+    mate = 2 * outer + (1 - inner)
+    t_near, t_far = t + 1 - 2 * (t % 2), lax.rem(t + n_tp // 2, n_tp)
+    t_cross = lax.rem(t_near + n_tp // 2, n_tp)
+    rows = bi.shape[1] // n
+    tokens = bi.shape[0]
+    cols = bi.shape[1] // n_tp
+    chans = mo_ref.shape[1]
+    chunks = xs.shape[0]
+    step = tokens // chunks
+
+    loads = []
+    for i, (src, dst) in enumerate(((bi_hbm, bi), (wv_hbm, wv), (wg_hbm, wg), (og_hbm, og))):
+        loads.append(pltpu.make_async_copy(src, dst, load_sem.at[i]))
+        loads[-1].start()
+
+    barrier = pltpu.get_barrier_semaphore()
+    peers = [{"sp": 2 * lax.rem(outer + k, h) + inner} for k in range(1, h)]
+    for who in peers + [{"sp": mate}, {"tp": t_near}, {"tp": t_far}]:
+        pl.semaphore_signal(barrier, inc=1, device_id=who, device_id_type=MESH)
+    pl.semaphore_wait(barrier, len(peers) + 3)
+
+    def send(src, dst, send_sem, recv_sem, who):
+        copy = pltpu.make_async_remote_copy(
+            src_ref=src, dst_ref=dst, send_sem=send_sem, recv_sem=recv_sem,
+            device_id=who, device_id_type=MESH,
+        )
+        copy.start()
+        return copy
+
+    small_copy = send(small_ref, small_in, s_send.at[0], s_recv.at[0], {"sp": mate})
+
+    aligned = rows % 128 == 0
+    wide = 256
+    def block_rows(o, i):
+        return pl.ds(pl.multiple_of((2 * o + i) * rows, rows), rows)
+
+    def product(act, other, where):
+        return lax.dot_general(
+            act[:, where], other[...], (((0,), (0,)), ((), ())),
+            preferred_element_type=jnp.float32,
+        ).astype(jnp.bfloat16)
+
+    def make_block(store, act, other, o, i):
+        if aligned:
+            store[block_rows(o, i), :] = product(act, other, block_rows(o, i))
+
+    def make_all(store, act, other):
+        if not aligned:
+            for c in range(act.shape[1] // wide):
+                where = pl.ds(c * wide, wide)
+                store[where, :] = product(act, other, where)
+
+    def partial_input(r, j):
+        at = pl.ds(pl.multiple_of(j * cols, cols), cols)
+        token = pl.ds(r * step, step)
+        return right_product(gb_ref[token, :chans], wv[at, :]) + right_product(
+            gb_ref[token, chans:], wg[at, :]
+        )
+
+    order = [lax.rem(outer + k, h) for k in range(1, h)] + [outer]
+
+    def near_block(r):
+        xs[r, 0] = partial_input(r, t_near).astype(jnp.bfloat16)
+        xs[r, 1] = partial_input(r, t_cross).astype(jnp.bfloat16)
+        return send(xs.at[r], xr.at[r], x_send.at[r], x_recv.at[r], {"tp": t_near})
+
+    def far_block(r):
+        mine = partial_input(r, t)
+        far = partial_input(r, t_far)
+        x_copies[r].wait_recv()
+        ys[r] = (far + xr[r, 1].astype(jnp.float32)).astype(jnp.bfloat16)
+        acc[pl.ds(r * step, step), :] = mine + xr[r, 0].astype(jnp.float32)
+        return send(ys.at[r], yr.at[r], y_send.at[r], y_recv.at[r], {"tp": t_far})
+
+    loads[0].wait()
+    make_all(gs, bi, gb_ref)
+    g_copies = []
+    x_copies = []
+    y_copies = []
+
+    def g_block(k):
+        o = order[k]
+        make_block(gs, bi, gb_ref, o, 1 - inner)
+        where = block_rows(o, 1 - inner)
+        g_copies.append(send(gs.at[where], gr.at[k], gs_send.at[k], gs_recv.at[k], {"sp": mate}))
+
+    g_block(0)
+    loads[1].wait()
+    loads[2].wait()
+    x_copies.append(near_block(0))
+    g_block(1)
+    x_copies.append(near_block(1))
+    y_copies.append(far_block(0))
+    loads[3].wait()
+    make_all(pm, og, mo_ref)
+    p_copies = []
+    for k in range(h - 1):
+        o = order[k]
+        for i in range(2):
+            make_block(pm, og, mo_ref, o, i)
+        where = pl.ds(pl.multiple_of(2 * o * rows, 2 * rows), 2 * rows)
+        p_copies.append(send(pm.at[where], pr.at[k], pr_send.at[k], pr_recv.at[k], {"sp": 2 * o + inner}))
+        if k + 2 < h:
+            g_block(k + 2)
+    for r in range(2, chunks):
+        x_copies.append(near_block(r))
+        y_copies.append(far_block(r - 1))
+    y_copies.append(far_block(chunks - 1))
+    for i in range(2):
+        make_block(pm, og, mo_ref, outer, i)
+    small_copy.wait()
+    small_pair[...] = small_ref[...] + small_in[...]
+    sa_copies = [
+        send(small_pair, small_all.at[outer], sa_send.at[k - 1], sa_recv.at[k - 1],
+             {"sp": 2 * lax.rem(outer + k, h) + inner})
+        for k in range(1, h)
+    ]
+    q_copies = []
+    for k in range(h):
+        o = order[k]
+        make_block(gs, bi, gb_ref, o, inner)
+        g_copies[k].wait_recv()
+        total = gs[block_rows(o, inner), :].astype(jnp.float32) + gr[k].astype(jnp.float32)
+        if k < h - 1:
+            gs2[k] = total.astype(jnp.bfloat16)
+            q_copies.append(send(gs2.at[k], gq.at[k], gq_send.at[k], gq_recv.at[k], {"sp": 2 * o + inner}))
+        else:
+            ws_ref[...] = total
+    for copy in p_copies:
+        copy.wait_recv()
+
+    def proj_total(i):
+        total = pm[block_rows(outer, i), :].astype(jnp.float32)
+        for k in range(h - 1):
+            total = total + pr[k, pl.ds(pl.multiple_of(i * rows, rows), rows), :].astype(jnp.float32)
+        return total
+
+    ps2[...] = proj_total(1 - inner).astype(jnp.bfloat16)
+    last = send(ps2, pq, pq_send.at[0], pq_recv.at[0], {"sp": mate})
+    ps_ref[...] = proj_total(inner)
+    for copy in sa_copies:
+        copy.wait_recv()
+    small_all[outer] = small_pair[...]
+    total = small_all[0]
+    for k in range(1, h):
+        total = total + small_all[k]
+    sm_ref[...] = total * loss_scale
+    for r in range(chunks):
+        y_copies[r].wait_recv()
+        token = pl.ds(r * step, step)
+        ig_ref[token, :] = (acc[token, :] + yr[r].astype(jnp.float32)).astype(jnp.bfloat16)
+    for copy in q_copies:
+        copy.wait_recv()
+    total = ws_ref[...]
+    for k in range(h - 1):
+        total = total + gq[k].astype(jnp.float32)
+    ws_ref[...] = total * loss_scale
+    last.wait_recv()
+    ps_ref[...] = (ps_ref[...] + pq[...].astype(jnp.float32)) * loss_scale
+    for copy in g_copies + x_copies + y_copies + p_copies + q_copies + sa_copies + [last]:
+        copy.wait_send()
+
+
+def tail(block_input, out_grad, w_value, w_gate, grad_both, mixer_out, small, loss_scale):
+    n, n_tp = lax.axis_size("sp"), lax.axis_size("tp")
+    tokens, width = block_input.shape
+    chans = mixer_out.shape[1]
+    rows, cols, h, chunks = width // n, width // n_tp, n // 2, 4
+    step = tokens // chunks
+    bf, f32 = jnp.bfloat16, jnp.float32
+    anywhere = pl.BlockSpec(memory_space=pl.ANY)
+    vmem = pl.BlockSpec(memory_space=pltpu.VMEM)
+    dma = pltpu.SemaphoreType.DMA
+    V = pltpu.VMEM
+    return pl.pallas_call(
+        functools.partial(tail_kernel, n, n_tp, loss_scale),
+        out_shape=(
+            jax.ShapeDtypeStruct((tokens, cols), bf),
+            jax.ShapeDtypeStruct((rows, 2 * chans), f32),
+            jax.ShapeDtypeStruct((rows, chans), f32),
+            jax.ShapeDtypeStruct(small.shape, f32),
+        ),
+        in_specs=[anywhere] * 4 + [vmem] * 3,
+        out_specs=(vmem,) * 4,
+        scratch_shapes=[
+            V((tokens, width), bf), V((tokens, width), bf), V((width, chans), bf), V((width, chans), bf),
+            V((width, 2 * chans), bf), V((h, rows, 2 * chans), bf), V((h - 1, rows, 2 * chans), bf),
+            V((h - 1, rows, 2 * chans), bf),
+            V((width, chans), bf), V((h - 1, 2 * rows, chans), bf), V((rows, chans), bf), V((rows, chans), bf),
+            V((chunks, 2, step, cols), bf), V((chunks, 2, step, cols), bf), V((chunks, step, cols), bf),
+            V((chunks, step, cols), bf), V((tokens, cols), f32),
+            V(small.shape, f32), V(small.shape, f32), V((h,) + small.shape, f32),
+            dma((4,)),
+            dma((h,)), dma((h,)), dma((h - 1,)), dma((h - 1,)), dma((h - 1,)), dma((h - 1,)), dma((1,)), dma((1,)),
+            dma((chunks,)), dma((chunks,)), dma((chunks,)), dma((chunks,)), dma((1,)), dma((1,)),
+            dma((h - 1,)), dma((h - 1,)),
+        ],
+        compiler_params=pltpu.CompilerParams(
+            collective_id=0, has_side_effects=True, vmem_limit_bytes=60 * 1024 * 1024
+        ),
+    )(block_input, out_grad, w_value, w_gate, grad_both, mixer_out, small)
 
 
 def shards(block_input, out_grad, w_value, w_gate, conv_taps, norm_gain, norm_shift, w_proj):
@@ -89,32 +312,19 @@
     grad_value = (grad_glu * gate_sigmoid).astype(jnp.bfloat16)
     grad_gate = (grad_glu * value_wide * gate_sigmoid * (1.0 - gate_sigmoid)).astype(jnp.bfloat16)
     grad_both = jnp.concatenate([grad_value, grad_gate], axis=1)
-    small_taps, small_gain, small_shift = lax.psum((taps_part, gain_part, shift_part), "sp")
-    partial_input = right_product(grad_value, w_value) + right_product(grad_gate, w_gate)
-    input_grad = lax.psum_scatter(
-        partial_input.astype(jnp.bfloat16), "tp", scatter_dimension=1, tiled=True
-    )
-    summed = lax.psum_scatter(
-        jnp.concatenate(
-            [column_product(block_input, grad_both), column_product(out_grad, mixer_out)], axis=1
-        ),
-        "sp",
-        scatter_dimension=0,
-        tiled=True,
-    )
-    weight_sum = summed[:, : 2 * channels_dev]
-    proj_sum = summed[:, 2 * channels_dev :]
-    value_wgrad = weight_sum[:, :channels_dev] * loss_scale
-    gate_wgrad = weight_sum[:, channels_dev:] * loss_scale
-    proj_wgrad = (proj_sum * loss_scale).T
+    small = jnp.concatenate([taps_part, gain_part[None], shift_part[None]], axis=0)
+    small = jnp.pad(small, ((0, -small.shape[0] % 8), (0, 0)))
+    input_grad, weight_sum, proj_sum, small_sum = tail(
+        block_input, out_grad, w_value, w_gate, grad_both, mixer_out, small, loss_scale
+    )
     return (
         input_grad,
-        value_wgrad,
-        gate_wgrad,
-        proj_wgrad,
-        small_taps * loss_scale,
-        small_gain * loss_scale,
-        small_shift * loss_scale,
+        weight_sum[:, :channels_dev],
+        weight_sum[:, channels_dev:],
+        proj_sum.T,
+        small_sum[:kernel_len],
+        small_sum[kernel_len],
+        small_sum[kernel_len + 1],
     )
 
 

time: 240 us -> 122 us (0.51)
  waiting for transfers between devices: 127 us -> 2.17 us
  Pallas kernels: 0 us -> 62.9 us
  blocking collectives: 43.3 us -> 12.8 us
  between operations: 14.4 us -> 0.86 us
  matrix products: 21.3 us -> 11 us
  local copies, waits for them, and re-layouts: 3.64 us -> 8.47 us
  other arithmetic: 22.9 us -> 18.4 us
    reduce_scatter x2 -> x0, waiting for transfers between devices: 124 us -> none  [the longest x1 80.4 us: shards(): lax.psum_scatter(jnp.concatenate([column_product(block_input, grad_both),...]
    pallas_call x0 -> x1, Pallas kernels: none -> 62.9 us  [tail(): pl.pallas_call(functools.partial(tail_kernel, n, n_tp, loss_scale), out_s...]
    psum x1 -> x0, blocking collectives: 30.5 us -> none  [shards(): lax.psum((taps_part, gain_part, shift_part), 'sp')]
    dot_general x3 -> x1, matrix products: 11.3 us -> 4.83 us  [right_product(): lax.dot_general(left, right, (((1,), (1,)), ((), ())), preferred_element_...]
    slice x0 -> x3, local copies, waits for them, and re-layouts: none -> 4.59 us  [the longest x1 1.85 us: shards(): weight_sum[:, channels_dev:]]
    dot_general x2 -> x0, matrix products: 3.91 us -> none  [column_product(): lax.dot_general(left, right, (((0,), (0,)), ((), ())), preferred_element_...]
  transfers between devices with their start and end apart: 4 -> 2, of which waited for: 4 -> 1; matrix products, arithmetic and copies ran while one was open for 6% -> 2% of each run, Pallas kernels for 0% -> 0%
where the time goes in v1:
time: 122 us
  Pallas kernels  62.9 us (52%)
  other arithmetic  18.4 us (15%)
  blocking collectives  12.8 us (10%)
  matrix products  11 us (9%)
  local copies, waits for them, and re-layouts  8.47 us (7%)
  starting transfers between devices  5.47 us (4%)
  waiting for transfers between devices  2.17 us (2%)
    pallas_call x1, Pallas kernels, tail(): pl.pallas_call(functools.partial(tail_kernel, n, n_tp, loss_scale), out_s...  62.9 us
    psum x1, blocking collectives, shards(): lax.psum((jnp.sum(filtered, axis=1), jnp.sum(filtered * filtered, axis=1)...  6.92 us
    reduce_sum x2, other arithmetic, shards(): jnp.sum(grad_filtered * extended[begin:begin + tok_rows], axis=0)  6.07 us
    psum x1, blocking collectives, shards(): lax.psum((jnp.sum(grad_normed, axis=1), jnp.sum(grad_normed * normed, axi...  5.85 us
    ppermute x2, starting transfers between devices, from_behind(): return lax.ppermute(block, axis, route)  5.47 us
    add x1, other arithmetic, shards(): grad_extended + conv_taps[tap_index] * padded_grad[tap_index:tap_index +...  4.89 us
    dot_general x1, matrix products, right_product(): lax.dot_general(left, right, (((1,), (1,)), ((), ())), preferred_element_...  4.83 us
    reduce_sum x1, other arithmetic, shards(): jnp.sum(filtered * filtered, axis=1)  4.65 us
  transfers between devices with their start and end apart: 2, of which 1 were waited for; matrix products, arithmetic and copies ran while one was open for 2% of the time, Pallas kernels for 0%

profile of v1, /device:TPU:9, one launch (start us, length us, event | category | flops | bytes accessed | tf_op | source)
XLA Modules:
  0.0 122.0 jit_solution(15503223437446943897)
XLA Ops:
  0.6 0.0 copy-start
  0.6 0.0 copy-start.1
  0.7 0.0 copy-start.2
  0.7 3.9 %convolution_convert_fusion.1 = bf16[1024,256]{1,0:T(8,128)(2,1)S(1)} fusion(bf16[1024,2048]{1,0:T(8,128)(2,1)} %bi_hbm.1, bf16[2048,256]{1,0:T(8,128)(2,1)} %wv_hbm.1), kind=kOutput, calls=%fused_computation.10 | convolution fusion | flops 1074003968 | bytes 5767168 | tf_op jit(solution)/shard_map/dot_general | solution.py:261
  4.6 0.0 copy-done.1
  4.6 0.2 copy-done.2
  4.8 0.0 copy-start.4
  4.8 0.0 copy-start.5
  4.8 2.3 %fusion.6 = (bf16[1024,256]{1,0:T(8,128)(2,1)S(1)}, f32[1024,256]{1,0:T(8,128)}) fusion(bf16[1024,256]{1,0:T(8,128)(2,1)S(1)} %convolution_convert_fusion.1, bf16[1024,2048]{1,0:T(8,128)(2,1)S(1)} %copy-done.1, bf16[2048,256]{1,0:T(8,128)(2,1)S(1)} %copy-done.2), kind=kOutput, calls=%fused_computation.12 | convolution fusion | flops 1075838976 | bytes 7340032 | tf_op jit(solution)/shard_map/dot_general | solution.py:264
  7.1 0.0 copy-done.4
  7.1 3.1 %collective-permute-start = (bf16[30,256]{1,0:T(8,128)(2,1)S(1)}, bf16[30,256]{1,0:T(8,128)(2,1)S(1)}, u32[]{:S(2)}, u32[]{:S(2)}) collective-permute-start(bf16[30,256]{1,0:T(8,128)(2,1)S(1)} %slice.470), channel_id=1, source_target_pairs={{0,4},{4,8},{8,12},{12,16},{16,20},{20,24},{24,28},{1,5},{5,9},{9,... | collective-permute-start | bytes 46088 | tf_op jit(solution)/shard_map/ppermute | solution.py:20
  10.2 0.0 copy-done.5
  10.3 2.2 %collective-permute-done = bf16[30,256]{1,0:T(8,128)(2,1)S(1)} collective-permute-done((bf16[30,256]{1,0:T(8,128)(2,1)S(1)}, bf16[30,256]{1,0:T(8,128)(2,1)S(1)}, u32[]{:S(2)}, u32[]{:S(2)}) %collective-permute-start) | collective-permute-done | bytes 15392 | tf_op jit(solution)/shard_map/ppermute | solution.py:20
  12.5 0.1 maximum_convert_fusion
  12.6 0.0 copy-start.6
  12.6 0.0 copy-start.7
  12.6 4.6 %multiply_reduce_fusion.33 = (f32[1024]{0:T(1024)S(1)}, f32[1024]{0:T(1024)S(1)}, f32[1024,256]{1,0:T(8,128)S(1)}) fusion(f32[1054,256]{1,0:T(8,128)S(1)} %maximum_convert_fusion, f32[256]{0:T(256)S(1)} %bitcast.132, f32[256]{0:T(256)S(1)} %bitcast.134, f32[256]{0:T(256)S(1)} %bitcast.76, f32[256]{0:T(256)S(1)} %bitcast.78, f32[256]{0:T(256)S(1)} %bitcast.80, ...), kind=kLoop, calls=%fused_computation.57 | loop fusion | flops 16775168 | bytes 33594368 | tf_op jit(solution)/shard_map/reduce_sum | solution.py:277
  17.2 6.9 %all-reduce.3 = (f32[1024]{0:T(1024)S(1)}, f32[1024]{0:T(1024)S(1)}) all-reduce(f32[1024]{0:T(1024)S(1)} %get-tuple-element.58, f32[1024]{0:T(1024)S(1)} %get-tuple-element.57), channel_id=1, replica_groups=mesh['sp'=8,'tp'=4] {'tp'}, use_global_device_ids=true, to_apply=%region_3.0 | all-reduce | flops 2048 | bytes 16384 | tf_op jit(solution)/shard_map/psum | solution.py:276
  24.2 0.0 copy-done
  24.2 0.0 copy-done.6
  24.2 0.0 copy-done.7
  24.2 4.8 %multiply_reduce_fusion = (f32[256]{0:T(256)S(1)}, f32[1024]{0:T(1024)S(1)}, f32[1024]{0:T(1024)S(1)}, f32[256]{0:T(256)S(1)}, bf16[1024,256]{1,0:T(8,128)(2,1)}, /*index=5*/f32[1024,256]{1,0:T(8,128)}) fusion(f32[1024,256]{1,0:T(8,128)S(1)} %get-tuple-element.64, f32[1024]{0:T(1024)S(1)} %get-tuple-element.104, f32[1024]{0:T(1024)S(1)} %get-tuple-element.103, ...), kind=kOutput, calls=%fused_computation.18 | convolution fusion | flops 1079244288 | bytes 7884800 | tf_op jit(solution)/shard_map/dot_general | solution.py:24
  29.1 5.9 %all-reduce.2 = (f32[1024]{0:T(1024)S(1)}, f32[1024]{0:T(1024)S(1)}) all-reduce(f32[1024]{0:T(1024)S(1)} %get-tuple-element.54, f32[1024]{0:T(1024)S(1)} %get-tuple-element.55), channel_id=1, replica_groups=mesh['sp'=8,'tp'=4] {'tp'}, use_global_device_ids=true, to_apply=%region_7.0 | all-reduce | flops 2048 | bytes 16384 | tf_op jit(solution)/shard_map/psum | solution.py:289
  34.9 4.3 %multiply_reduce_fusion.1 = (f32[256]{0:T(256)S(1)}, f32[256]{0:T(256)S(1)}, f32[256]{0:T(256)S(1)}, f32[256]{0:T(256)S(1)}, f32[256]{0:T(256)S(1)}, /*index=5*/...) fusion(f32[1054,256]{1,0:T(8,128)S(1)} %maximum_convert_fusion,, ...), kind=kLoop, calls=%fused_computation.19 | loop fusion | flops 11267584 | bytes 22055936 | tf_op jit(solution)/shard_map/reduce_sum | solution.py:306
  39.2 4.9 %multiply_add_fusion = f32[1054,256]{1,0:T(8,128)S(1)} fusion(f32[1024,256]{1,0:T(8,128)S(1)} %get-tuple-element.63, f32[256]{0:T(256)S(1)} %bitcast.133, f32[256]{0:T(256)S(1)} %bitcast.135, f32[256]{0:T(256)S(1)} %bitcast.77, f32[256]{0:T(256)S(1)} %bitcast.79, f32[256]{0:T(256)S(1)} %bitcast.81, f32[256]{0:T(256)S(1)} %bitcast.83, f32[256]{0:T(256)S(1)} %bitcast.85, ...), kind=kLoop, calls=%fused_computation.11 | loop fusion | flops 16459264 | bytes 2159616 | tf_op jit(solution)/shard_map/add | solution.py:303
  44.2 2.3 %collective-permute-start.1 = (f32[30,256]{1,0:T(8,128)S(1)}, f32[30,256]{1,0:T(8,128)S(1)}, u32[]{:S(2)}, u32[]{:S(2)}) collective-permute-start(f32[30,256]{1,0:T(8,128)S(1)} %slice.504), channel_id=1, source_target_pairs={{4,0},{8,4},{12,8},{16,12},{20,16},{24,20},{28,24},{5,1},{9,5},{13... | collective-permute-start | bytes 92168 | tf_op jit(solution)/shard_map/ppermute | solution.py:20
  46.5 1.8 %multiply_reduce_fusion.19 = (f32[256]{0:T(256)S(1)}, f32[256]{0:T(256)S(1)}, f32[256]{0:T(256)S(1)}, f32[256]{0:T(256)S(1)}, f32[256]{0:T(256)S(1)}, /*index=5*...) fusion(f32[1024,256]{1,0:T(8,128)S(1)} %get-tuple-element.63, ...), kind=kLoop, calls=%fused_computation.37 | loop fusion | flops 6812416 | bytes 14693376 | tf_op jit(solution)/shard_map/reduce_sum | solution.py:306
  48.2 0.1 slice.502
  48.3 0.1 concatenate.15
  48.4 0.6 pad.9.small_ref
  49.1 0.0 collective-permute-done.1
  49.1 1.6 %multiply_convert_fusion.1 = (bf16[1024,256]{1,0:T(8,128)(2,1)S(1)}, bf16[1024,256]{1,0:T(8,128)(2,1)S(1)}) fusion(f32[1024,256]{1,0:T(8,128)} %get-tuple-element.106, f32[30,256]{1,0:T(8,128)S(1)} %slice_add_fusion, f32[994,256]{1,0:T(8,128)S(1)} %slice.502, bf16[1024,256]{1,0:T(8,128)(2,1)} %copy-done.4), kind=kLoop, calls=%fused_computation.51 | loop fusion | flops 2359296 | bytes 3670016 | tf_op jit(solution)/shard_map/convert_element_type | solution.py:312
  50.7 1.1 pad_maximum_fusion.1.gb_ref
  51.8 62.9 %shard_map.135 = (bf16[1024,512]{1,0:T(8,128)(2,1)}, f32[256,512]{1,0:T(8,128)}, f32[256,256]{1,0:T(8,128)}, f32[40,256]{1,0:T(8,128)}) custom-call(bf16[1024,2048]{1,0:T(8,128)(2,1)} %bi_hbm.1, bf16[1024,2048]{1,0:T(8,128)(2,1)} %og_hbm.1, bf16[2048,256]{1,0:T(8,128)(2,1)} %wv_hbm.1, bf16[2048,256]{1,0:T(8,128)(2,1)} %wg_hbm.1, ...), custom_call_target="tpu_custom_call" | custom-call | tf_op jit(solution)/shard_map/pallas_call | solution.py:226
  114.7 0.0 copy-start.3
  114.7 1.4 %fusion.11 = (f32[1,256]{1,0:T(1,128)}, f32[1,256]{1,0:T(1,128)}) fusion(f32[40,256]{1,0:T(8,128)} %get-tuple-element.14), kind=kLoop, calls=%fused_computation.67 | loop fusion | bytes 4096 | tf_op jit(solution)/shard_map/slice | solution.py:327
  116.0 1.4 %slice.467 = f32[31,256]{1,0:T(8,128)} slice(f32[40,256]{1,0:T(8,128)} %get-tuple-element.14), slice={[0:31], [0:256]} | slice | bytes 63488 | tf_op jit(solution)/shard_map/slice | solution.py:325
  117.4 1.8 %copy.15 = f32[256,256]{1,0:T(8,128)} copy(f32[256,256]{0,1:T(8,128)} %bitcast.73) | data formatting | bytes 524288
  119.2 1.9 %fusion.10 = (f32[256,256]{1,0:T(8,128)}, f32[256,256]{1,0:T(8,128)}) fusion(f32[256,512]{1,0:T(8,128)} %get-tuple-element.12), kind=kLoop, calls=%fused_computation.66 | loop fusion | bytes 1048576 | tf_op jit(solution)/shard_map/slice | solution.py:323
  121.1 0.0 copy-done.3
  121.1 1.0 copy.17
  (7 shorter events, 0.1 us)
Async XLA Ops:
  0.6 23.6 %copy-start = (bf16[256,2048]{1,0:T(8,128)(2,1)S(1)}, bf16[256,2048]{1,0:T(8,128)(2,1)}, u32[]{:S(2)}) copy-start(bf16[256,2048]{1,0:T(8,128)(2,1)} %param.15) | copy-start | bytes 3145732
  0.6 3.9 %copy-start.1 = (bf16[1024,2048]{1,0:T(8,128)(2,1)S(1)}, bf16[1024,2048]{1,0:T(8,128)(2,1)}, u32[]{:S(2)}) copy-start(bf16[1024,2048]{1,0:T(8,128)(2,1)} %bi_hbm.1) | copy-start | bytes 12582916
  0.7 4.1 %copy-start.2 = (bf16[2048,256]{1,0:T(8,128)(2,1)S(1)}, bf16[2048,256]{1,0:T(8,128)(2,1)}, u32[]{:S(2)}) copy-start(bf16[2048,256]{1,0:T(8,128)(2,1)} %wg_hbm.1) | copy-start | bytes 3145732
  4.8 2.3 %copy-start.4 = (bf16[1024,256]{1,0:T(8,128)(2,1)}, bf16[1024,256]{1,0:T(8,128)(2,1)S(1)}, u32[]{:S(2)}) copy-start(bf16[1024,256]{1,0:T(8,128)(2,1)S(1)} %convolution_convert_fusion.1) | copy-start | bytes 1572868
  4.8 5.4 %copy-start.5 = (f32[31,256]{1,0:T(8,128)S(1)}, f32[31,256]{1,0:T(8,128)}, u32[]{:S(2)}) copy-start(f32[31,256]{1,0:T(8,128)} %param.12) | copy-start | bytes 95236
  7.1 5.4 %collective-permute-start = (bf16[30,256]{1,0:T(8,128)(2,1)S(1)}, bf16[30,256]{1,0:T(8,128)(2,1)S(1)}, u32[]{:S(2)}, u32[]{:S(2)}) collective-permute-start(bf16[30,256]{1,0:T(8,128)(2,1)S(1)} %slice.470), channel_id=1, source_target_pairs={{0,4},{4,8},{8,12},{12,16},{16,20},{20,24},{24,28},{1,5},{5,9},{9,... | collective-permute-start | bytes 46088 | tf_op jit(solution)/shard_map/ppermute | solution.py:20
  12.6 11.6 %copy-start.6 = (f32[256]{0:T(256)S(1)}, f32[256]{0:T(256)}, u32[]{:S(2)}) copy-start(f32[256]{0:T(256)} %param.13) | copy-start | bytes 3076
  12.6 11.6 %copy-start.7 = (f32[256]{0:T(256)S(1)}, f32[256]{0:T(256)}, u32[]{:S(2)}) copy-start(f32[256]{0:T(256)} %param.14) | copy-start | bytes 3076
  44.2 4.9 %collective-permute-start.1 = (f32[30,256]{1,0:T(8,128)S(1)}, f32[30,256]{1,0:T(8,128)S(1)}, u32[]{:S(2)}, u32[]{:S(2)}) collective-permute-start(f32[30,256]{1,0:T(8,128)S(1)} %slice.504), channel_id=1, source_target_pairs={{4,0},{8,4},{12,8},{16,12},{20,16},{24,20},{28,24},{5,1},{9,5},{13... | collective-permute-start | bytes 92168 | tf_op jit(solution)/shard_map/ppermute | solution.py:20
  114.7 6.4 %copy-start.3 = (bf16[1024,512]{1,0:T(8,128)(2,1)S(1)}, bf16[1024,512]{1,0:T(8,128)(2,1)}, u32[]{:S(2)}) copy-start(bf16[1024,512]{1,0:T(8,128)(2,1)} %get-tuple-element.117) | copy-start | bytes 3145732

commit v2 on v1

--- a/solution.py
+++ b/solution.py
@@ -37,12 +37,11 @@
 
 def tail_kernel(
     n, n_tp, loss_scale,
-    bi_hbm, og_hbm, wv_hbm, wg_hbm, gb_ref, mo_ref, small_ref,
-    ig_ref, ws_ref, ps_ref, sm_ref,
-    bi, og, wv, wg,
+    bi, og_hbm, wv, wg, gb_ref, mo_ref, small_ref,
+    ig_ref, wv_out, wg_out, ps_out, taps_out, gain_out, shift_out,
+    ws_ref, ps_ref, og, og_sem,
     gs, gr, gs2, gq, pm, pr, ps2, pq,
     xs, xr, ys, yr, acc, small_pair, small_in, small_all,
-    load_sem,
     gs_send, gs_recv, gq_send, gq_recv, pr_send, pr_recv, pq_send, pq_recv,
     x_send, x_recv, y_send, y_recv, s_send, s_recv, sa_send, sa_recv,
 ):
@@ -59,10 +58,8 @@
     chunks = xs.shape[0]
     step = tokens // chunks
 
-    loads = []
-    for i, (src, dst) in enumerate(((bi_hbm, bi), (wv_hbm, wv), (wg_hbm, wg), (og_hbm, og))):
-        loads.append(pltpu.make_async_copy(src, dst, load_sem.at[i]))
-        loads[-1].start()
+    og_load = pltpu.make_async_copy(og_hbm, og, og_sem.at[0])
+    og_load.start()
 
     barrier = pltpu.get_barrier_semaphore()
     peers = [{"sp": 2 * lax.rem(outer + k, h) + inner} for k in range(1, h)]
@@ -123,7 +120,6 @@
         acc[pl.ds(r * step, step), :] = mine + xr[r, 0].astype(jnp.float32)
         return send(ys.at[r], yr.at[r], y_send.at[r], y_recv.at[r], {"tp": t_far})
 
-    loads[0].wait()
     make_all(gs, bi, gb_ref)
     g_copies = []
     x_copies = []
@@ -136,13 +132,11 @@
         g_copies.append(send(gs.at[where], gr.at[k], gs_send.at[k], gs_recv.at[k], {"sp": mate}))
 
     g_block(0)
-    loads[1].wait()
-    loads[2].wait()
     x_copies.append(near_block(0))
     g_block(1)
     x_copies.append(near_block(1))
     y_copies.append(far_block(0))
-    loads[3].wait()
+    og_load.wait()
     make_all(pm, og, mo_ref)
     p_copies = []
     for k in range(h - 1):
@@ -195,7 +189,11 @@
     total = small_all[0]
     for k in range(1, h):
         total = total + small_all[k]
-    sm_ref[...] = total * loss_scale
+    total = total * loss_scale
+    taps = taps_out.shape[0]
+    taps_out[...] = total[:taps]
+    gain_out[...] = total[taps : taps + 1]
+    shift_out[...] = total[taps + 1 : taps + 2]
     for r in range(chunks):
         y_copies[r].wait_recv()
         token = pl.ds(r * step, step)
@@ -205,21 +203,22 @@
     total = ws_ref[...]
     for k in range(h - 1):
         total = total + gq[k].astype(jnp.float32)
-    ws_ref[...] = total * loss_scale
+    wv_out[...] = total[:, :chans] * loss_scale
+    wg_out[...] = total[:, chans:] * loss_scale
     last.wait_recv()
-    ps_ref[...] = (ps_ref[...] + pq[...].astype(jnp.float32)) * loss_scale
+    total = (ps_ref[...] + pq[...].astype(jnp.float32)) * loss_scale
+    ps_out[...] = total.T if aligned else total
     for copy in g_copies + x_copies + y_copies + p_copies + q_copies + sa_copies + [last]:
         copy.wait_send()
 
 
-def tail(block_input, out_grad, w_value, w_gate, grad_both, mixer_out, small, loss_scale):
+def tail(block_input, out_grad, w_value, w_gate, grad_both, mixer_out, small, taps, loss_scale):
     n, n_tp = lax.axis_size("sp"), lax.axis_size("tp")
     tokens, width = block_input.shape
     chans = mixer_out.shape[1]
     rows, cols, h, chunks = width // n, width // n_tp, n // 2, 4
     step = tokens // chunks
     bf, f32 = jnp.bfloat16, jnp.float32
-    anywhere = pl.BlockSpec(memory_space=pl.ANY)
     vmem = pl.BlockSpec(memory_space=pltpu.VMEM)
     dma = pltpu.SemaphoreType.DMA
     V = pltpu.VMEM
@@ -227,27 +226,29 @@
         functools.partial(tail_kernel, n, n_tp, loss_scale),
         out_shape=(
             jax.ShapeDtypeStruct((tokens, cols), bf),
-            jax.ShapeDtypeStruct((rows, 2 * chans), f32),
             jax.ShapeDtypeStruct((rows, chans), f32),
-            jax.ShapeDtypeStruct(small.shape, f32),
+            jax.ShapeDtypeStruct((rows, chans), f32),
+            jax.ShapeDtypeStruct((chans, rows) if rows % 128 == 0 else (rows, chans), f32),
+            jax.ShapeDtypeStruct((taps, chans), f32),
+            jax.ShapeDtypeStruct((1, chans), f32),
+            jax.ShapeDtypeStruct((1, chans), f32),
         ),
-        in_specs=[anywhere] * 4 + [vmem] * 3,
-        out_specs=(vmem,) * 4,
+        in_specs=[vmem, pl.BlockSpec(memory_space=pltpu.HBM)] + [vmem] * 5,
+        out_specs=(vmem,) * 7,
         scratch_shapes=[
-            V((tokens, width), bf), V((tokens, width), bf), V((width, chans), bf), V((width, chans), bf),
+            V((rows, 2 * chans), f32), V((rows, chans), f32), V((tokens, width), bf), dma((1,)),
             V((width, 2 * chans), bf), V((h, rows, 2 * chans), bf), V((h - 1, rows, 2 * chans), bf),
             V((h - 1, rows, 2 * chans), bf),
             V((width, chans), bf), V((h - 1, 2 * rows, chans), bf), V((rows, chans), bf), V((rows, chans), bf),
             V((chunks, 2, step, cols), bf), V((chunks, 2, step, cols), bf), V((chunks, step, cols), bf),
             V((chunks, step, cols), bf), V((tokens, cols), f32),
             V(small.shape, f32), V(small.shape, f32), V((h,) + small.shape, f32),
-            dma((4,)),
             dma((h,)), dma((h,)), dma((h - 1,)), dma((h - 1,)), dma((h - 1,)), dma((h - 1,)), dma((1,)), dma((1,)),
             dma((chunks,)), dma((chunks,)), dma((chunks,)), dma((chunks,)), dma((1,)), dma((1,)),
             dma((h - 1,)), dma((h - 1,)),
         ],
         compiler_params=pltpu.CompilerParams(
-            collective_id=0, has_side_effects=True, vmem_limit_bytes=60 * 1024 * 1024
+            collective_id=0, has_side_effects=True, vmem_limit_bytes=36 * 1024 * 1024
         ),
     )(block_input, out_grad, w_value, w_gate, grad_both, mixer_out, small)
 
@@ -314,17 +315,14 @@
     grad_both = jnp.concatenate([grad_value, grad_gate], axis=1)
     small = jnp.concatenate([taps_part, gain_part[None], shift_part[None]], axis=0)
     small = jnp.pad(small, ((0, -small.shape[0] % 8), (0, 0)))
-    input_grad, weight_sum, proj_sum, small_sum = tail(
-        block_input, out_grad, w_value, w_gate, grad_both, mixer_out, small, loss_scale
-    )
+    input_grad, value_wgrad, gate_wgrad, proj_wgrad, taps_grad, gain_grad, shift_grad = tail(
+        block_input, out_grad, w_value, w_gate, grad_both, mixer_out, small, kernel_len, loss_scale
+    )
+    if proj_wgrad.shape[0] != channels_dev:
+        proj_wgrad = proj_wgrad.T
     return (
-        input_grad,
-        weight_sum[:, :channels_dev],
-        weight_sum[:, channels_dev:],
-        proj_sum.T,
-        small_sum[:kernel_len],
-        small_sum[kernel_len],
-        small_sum[kernel_len + 1],
+        input_grad, value_wgrad, gate_wgrad, proj_wgrad, taps_grad,
+        gain_grad.reshape(channels_dev), shift_grad.reshape(channels_dev),
     )
 
 

time: 122 us -> 129 us (1.057)
  other arithmetic: 18.4 us -> 27 us
  Pallas kernels: 62.9 us -> 59.3 us
  local copies, waits for them, and re-layouts: 8.47 us -> 9.84 us
    reduce_sum x2, other arithmetic: 6.07 us -> 13.9 us  [shards(): jnp.sum(grad_filtered * extended[begin:begin + tok_rows], axis=0)]
    unnamed x18 -> x31, local copies, waits for them, and re-layouts: 3.02 us -> 8.63 us
    slice x3 -> x0, local copies, waits for them, and re-layouts: 4.59 us -> none  [the longest x1 1.85 us: shards(): weight_sum[:, channels_dev:]]
    pallas_call x1, Pallas kernels: 62.9 us -> 59.3 us  [tail(): pl.pallas_call(functools.partial(tail_kernel, n, n_tp, loss_scale), out_s...]
where the time goes in v2:
time: 129 us
  Pallas kernels  59.3 us (46%)
  other arithmetic  27 us (21%)
  blocking collectives  12.8 us (10%)
  matrix products  11.3 us (9%)
  local copies, waits for them, and re-layouts  9.84 us (8%)
  starting transfers between devices  5.47 us (4%)
  waiting for transfers between devices  2.17 us (2%)
    pallas_call x1, Pallas kernels, tail(): pl.pallas_call(functools.partial(tail_kernel, n, n_tp, loss_scale), out_s...  59.3 us
    reduce_sum x2, other arithmetic, shards(): jnp.sum(grad_filtered * extended[begin:begin + tok_rows], axis=0)  13.9 us
    unnamed x31, local copies, waits for them, and re-layouts  8.63 us
    psum x1, blocking collectives, shards(): lax.psum((jnp.sum(filtered, axis=1), jnp.sum(filtered * filtered, axis=1)...  6.9 us
    psum x1, blocking collectives, shards(): lax.psum((jnp.sum(grad_normed, axis=1), jnp.sum(grad_normed * normed, axi...  5.85 us
    ppermute x2, starting transfers between devices, from_behind(): return lax.ppermute(block, axis, route)  5.47 us
    reduce_sum x1, other arithmetic, shards(): jnp.sum(filtered * filtered, axis=1)  5.24 us
    dot_general x1, matrix products, right_product(): lax.dot_general(left, right, (((1,), (1,)), ((), ())), preferred_element_...  5.12 us
  transfers between devices with their start and end apart: 2, of which 1 were waited for; matrix products, arithmetic and copies ran while one was open for 2% of the time, Pallas kernels for 0%

profile of v2, /device:TPU:9, one launch (start us, length us, event | category | flops | bytes accessed | tf_op | source)
XLA Modules:
  0.0 128.7 jit_solution(2273292217935513319)
XLA Ops:
  0.6 0.0 copy-start
  0.6 0.0 copy-start.1
  0.7 0.0 copy-start.5
  0.7 3.9 %convolution_convert_fusion.1 = bf16[1024,256]{1,0:T(8,128)(2,1)S(1)} fusion(bf16[1024,2048]{1,0:T(8,128)(2,1)} %bi.1, bf16[2048,256]{1,0:T(8,128)(2,1)} %wv.1), kind=kOutput, calls=%fused_computation.10 | convolution fusion | flops 1074003968 | bytes 5767168 | tf_op jit(solution)/shard_map/dot_general | solution.py:262
  4.6 0.0 copy-done.1
  4.6 0.2 copy-done.5
  4.8 0.0 copy-start.9
  4.8 2.3 %fusion.6 = (bf16[1024,256]{1,0:T(8,128)(2,1)S(1)}, f32[1024,256]{1,0:T(8,128)}) fusion(bf16[1024,256]{1,0:T(8,128)(2,1)S(1)} %convolution_convert_fusion.1, bf16[1024,2048]{1,0:T(8,128)(2,1)S(1)} %copy-done.1, bf16[2048,256]{1,0:T(8,128)(2,1)S(1)} %copy-done.5), kind=kOutput, calls=%fused_computation.12 | convolution fusion | flops 1075838976 | bytes 7340032 | tf_op jit(solution)/shard_map/dot_general | solution.py:265
  7.1 3.1 %collective-permute-start = (bf16[30,256]{1,0:T(8,128)(2,1)S(1)}, bf16[30,256]{1,0:T(8,128)(2,1)S(1)}, u32[]{:S(2)}, u32[]{:S(2)}) collective-permute-start(bf16[30,256]{1,0:T(8,128)(2,1)S(1)} %slice.450), channel_id=1, source_target_pairs={{0,4},{4,8},{8,12},{12,16},{16,20},{20,24},{24,28},{1,5},{5,9},{9,... | collective-permute-start | bytes 46088 | tf_op jit(solution)/shard_map/ppermute | solution.py:20
  10.2 0.0 copy-done.9
  10.3 2.2 %collective-permute-done = bf16[30,256]{1,0:T(8,128)(2,1)S(1)} collective-permute-done((bf16[30,256]{1,0:T(8,128)(2,1)S(1)}, bf16[30,256]{1,0:T(8,128)(2,1)S(1)}, u32[]{:S(2)}, u32[]{:S(2)}) %collective-permute-start) | collective-permute-done | bytes 15392 | tf_op jit(solution)/shard_map/ppermute | solution.py:20
  12.5 0.1 maximum_convert_fusion
  12.6 0.0 copy-start.6
  12.6 0.0 copy-start.10
  12.6 0.0 copy-start.11
  12.6 5.2 %multiply_reduce_fusion.33 = (f32[1024]{0:T(1024)S(1)}, f32[1024]{0:T(1024)S(1)}, f32[1024,256]{1,0:T(8,128)}) fusion(f32[1054,256]{1,0:T(8,128)S(1)} %maximum_convert_fusion, f32[256]{0:T(256)S(1)} %bitcast.132, f32[256]{0:T(256)S(1)} %bitcast.134, f32[256]{0:T(256)S(1)} %bitcast.76, f32[256]{0:T(256)S(1)} %bitcast.78, f32[256]{0:T(256)S(1)} %bitcast.80, ...), kind=kLoop, calls=%fused_computation.57 | loop fusion | flops 16775168 | bytes 33594368 | tf_op jit(solution)/shard_map/reduce_sum | solution.py:278
  17.8 0.0 copy-done.6
  17.8 6.9 %all-reduce.3 = (f32[1024]{0:T(1024)S(1)}, f32[1024]{0:T(1024)S(1)}) all-reduce(f32[1024]{0:T(1024)S(1)} %get-tuple-element.57, f32[1024]{0:T(1024)S(1)} %get-tuple-element.56), channel_id=1, replica_groups=mesh['sp'=8,'tp'=4] {'tp'}, use_global_device_ids=true, to_apply=%region_3.0 | all-reduce | flops 2048 | bytes 16384 | tf_op jit(solution)/shard_map/psum | solution.py:277
  24.8 0.0 copy-done
  24.8 0.0 copy-done.10
  24.8 0.0 copy-done.11
  24.8 5.1 %multiply_reduce_fusion = (f32[256]{0:T(256)S(1)}, f32[1024]{0:T(1024)S(1)}, f32[1024]{0:T(1024)S(1)}, f32[256]{0:T(256)S(1)}, bf16[1024,256]{1,0:T(8,128)(2,1)S(1)}, /*index=5*/f32[1024,256]{1,0:T(8,128)}) fusion(f32[1024,256]{1,0:T(8,128)} %get-tuple-element.63, f32[1024]{0:T(1024)S(1)} %get-tuple-element.99, f32[1024]{0:T(1024)S(1)} %get-tuple-element.98, ...), kind=kOutput, calls=%fused_computation.18 | convolution fusion | flops 1079244288 | bytes 7884800 | tf_op jit(solution)/shard_map/dot_general | solution.py:24
  29.9 5.9 %all-reduce.2 = (f32[1024]{0:T(1024)S(1)}, f32[1024]{0:T(1024)S(1)}) all-reduce(f32[1024]{0:T(1024)S(1)} %get-tuple-element.53, f32[1024]{0:T(1024)S(1)} %get-tuple-element.54), channel_id=1, replica_groups=mesh['sp'=8,'tp'=4] {'tp'}, use_global_device_ids=true, to_apply=%region_7.0 | all-reduce | flops 2048 | bytes 16384 | tf_op jit(solution)/shard_map/psum | solution.py:290
  35.8 12.2 %multiply_reduce_fusion.1 = (f32[256]{0:T(256)S(1)}, f32[256]{0:T(256)S(1)}, f32[256]{0:T(256)S(1)}, f32[256]{0:T(256)S(1)}, f32[256]{0:T(256)S(1)}, /*index=5*/...) fusion(f32[1054,256]{1,0:T(8,128)} %copy-done.6, ...), kind=kLoop, calls=%fused_computation.19 | loop fusion | flops 11267584 | bytes 22055936 | tf_op jit(solution)/shard_map/reduce_sum | solution.py:307
  48.0 0.0 copy-start.7
  48.0 4.9 %multiply_add_fusion = f32[1054,256]{1,0:T(8,128)S(1)} fusion(f32[1024,256]{1,0:T(8,128)S(1)} %get-tuple-element.62, f32[256]{0:T(256)S(1)} %bitcast.133, f32[256]{0:T(256)S(1)} %bitcast.135, f32[256]{0:T(256)S(1)} %bitcast.77, f32[256]{0:T(256)S(1)} %bitcast.79, f32[256]{0:T(256)S(1)} %bitcast.81, f32[256]{0:T(256)S(1)} %bitcast.83, f32[256]{0:T(256)S(1)} %bitcast.85, ...), kind=kLoop, calls=%fused_computation.11 | loop fusion | flops 16459264 | bytes 2159616 | tf_op jit(solution)/shard_map/add | solution.py:304
  52.9 0.0 copy-start.8
  52.9 2.3 %collective-permute-start.1 = (f32[30,256]{1,0:T(8,128)S(1)}, f32[30,256]{1,0:T(8,128)S(1)}, u32[]{:S(2)}, u32[]{:S(2)}) collective-permute-start(f32[30,256]{1,0:T(8,128)S(1)} %slice.484), channel_id=1, source_target_pairs={{4,0},{8,4},{12,8},{16,12},{20,16},{24,20},{28,24},{5,1},{9,5},{13... | collective-permute-start | bytes 92168 | tf_op jit(solution)/shard_map/ppermute | solution.py:20
  55.2 0.0 copy-done.7
  55.2 1.8 %multiply_reduce_fusion.19 = (f32[256]{0:T(256)S(1)}, f32[256]{0:T(256)S(1)}, f32[256]{0:T(256)S(1)}, f32[256]{0:T(256)S(1)}, f32[256]{0:T(256)S(1)}, /*index=5*...) fusion(f32[1024,256]{1,0:T(8,128)S(1)} %get-tuple-element.62, ...), kind=kLoop, calls=%fused_computation.37 | loop fusion | flops 6812416 | bytes 14693376 | tf_op jit(solution)/shard_map/reduce_sum | solution.py:307
  57.0 0.0 copy-done.8
  57.0 1.0 slice.482
  58.1 0.1 concatenate.15
  58.2 0.0 collective-permute-done.1
  58.2 0.8 slice_add_fusion
  59.0 0.0 copy-start.2
  59.0 1.9 %multiply_convert_fusion.1 = (bf16[1024,256]{1,0:T(8,128)(2,1)S(1)}, bf16[1024,256]{1,0:T(8,128)(2,1)S(1)}) fusion(f32[1024,256]{1,0:T(8,128)} %get-tuple-element.101, f32[30,256]{1,0:T(8,128)S(1)} %slice_add_fusion, f32[994,256]{1,0:T(8,128)} %slice.482, bf16[1024,256]{1,0:T(8,128)(2,1)S(1)} %convolution_convert_fusion.1), kind=kLoop, calls=%fused_computation.51 | loop fusion | flops 2359296 | bytes 3670016 | tf_op jit(solution)/shard_map/convert_element_type | solution.py:313
  60.9 0.0 copy-start.4
  60.9 0.1 pad_maximum_fusion.1.gb_ref
  61.0 0.8 copy-done.2
  61.8 0.6 copy-done.4
  62.3 0.0 copy-start.3
  62.3 2.2 %copy-done.3 = bf16[1024,2048]{1,0:T(8,128)(2,1)S(1)} copy-done((bf16[1024,2048]{1,0:T(8,128)(2,1)S(1)}, bf16[1024,2048]{1,0:T(8,128)(2,1)}, u32[]{:S(2)}) %copy-start.3) | copy-done | bytes 4194328
  64.5 59.3 %shard_map.135 = (bf16[1024,512]{1,0:T(8,128)(2,1)S(1)}, f32[256,256]{1,0:T(8,128)S(1)}, f32[256,256]{1,0:T(8,128)S(1)}, f32[256,256]{1,0:T(8,128)S(1)}, f32[31,...) custom-call(bf16[1024,2048]{1,0:T(8,128)(2,1)S(1)} %copy-done.2, bf16[1024,2048]{1,0:T(8,128)(2,1)S(1)} %copy-done.3, ...), custom_call_target="tpu_custom_call" | custom-call | tf_op jit(solution)/shard_map/pallas_call | solution.py:225
  123.9 1.0 copy.22
  124.8 0.7 copy.23
  125.5 0.7 copy.24
  126.2 0.7 copy.25
  126.9 0.6 copy.26
  127.6 0.6 copy.27
  128.1 0.6 copy.28
  (7 shorter events, 0.1 us)
Async XLA Ops:
  0.6 24.1 %copy-start = (bf16[256,2048]{1,0:T(8,128)(2,1)S(1)}, bf16[256,2048]{1,0:T(8,128)(2,1)}, u32[]{:S(2)}) copy-start(bf16[256,2048]{1,0:T(8,128)(2,1)} %param.15) | copy-start | bytes 3145732
  0.6 3.9 %copy-start.1 = (bf16[1024,2048]{1,0:T(8,128)(2,1)S(1)}, bf16[1024,2048]{1,0:T(8,128)(2,1)}, u32[]{:S(2)}) copy-start(bf16[1024,2048]{1,0:T(8,128)(2,1)} %bi.1) | copy-start | bytes 12582916
  0.7 4.1 %copy-start.5 = (bf16[2048,256]{1,0:T(8,128)(2,1)S(1)}, bf16[2048,256]{1,0:T(8,128)(2,1)}, u32[]{:S(2)}) copy-start(bf16[2048,256]{1,0:T(8,128)(2,1)} %wg.1) | copy-start | bytes 3145732
  4.8 5.4 %copy-start.9 = (f32[31,256]{1,0:T(8,128)S(1)}, f32[31,256]{1,0:T(8,128)}, u32[]{:S(2)}) copy-start(f32[31,256]{1,0:T(8,128)} %param.12) | copy-start | bytes 95236
  7.1 5.4 %collective-permute-start = (bf16[30,256]{1,0:T(8,128)(2,1)S(1)}, bf16[30,256]{1,0:T(8,128)(2,1)S(1)}, u32[]{:S(2)}, u32[]{:S(2)}) collective-permute-start(bf16[30,256]{1,0:T(8,128)(2,1)S(1)} %slice.450), channel_id=1, source_target_pairs={{0,4},{4,8},{8,12},{12,16},{16,20},{20,24},{24,28},{1,5},{5,9},{9,... | collective-permute-start | bytes 46088 | tf_op jit(solution)/shard_map/ppermute | solution.py:20
  12.6 5.3 %copy-start.6 = (f32[1054,256]{1,0:T(8,128)}, f32[1054,256]{1,0:T(8,128)S(1)}, u32[]{:S(2)}) copy-start(f32[1054,256]{1,0:T(8,128)S(1)} %maximum_convert_fusion) | copy-start | bytes 3237892
  12.6 12.2 %copy-start.10 = (f32[256]{0:T(256)S(1)}, f32[256]{0:T(256)}, u32[]{:S(2)}) copy-start(f32[256]{0:T(256)} %param.13) | copy-start | bytes 3076
  12.6 12.2 %copy-start.11 = (f32[256]{0:T(256)S(1)}, f32[256]{0:T(256)}, u32[]{:S(2)}) copy-start(f32[256]{0:T(256)} %param.14) | copy-start | bytes 3076
  48.0 7.2 %copy-start.7 = (f32[1054,256]{1,0:T(8,128)S(1)}, f32[1054,256]{1,0:T(8,128)}, u32[]{:S(2)}) copy-start(f32[1054,256]{1,0:T(8,128)} %copy-done.6) | copy-start | bytes 3237892
  52.9 4.1 %copy-start.8 = (f32[1054,256]{1,0:T(8,128)}, f32[1054,256]{1,0:T(8,128)S(1)}, u32[]{:S(2)}) copy-start(f32[1054,256]{1,0:T(8,128)S(1)} %multiply_add_fusion) | copy-start | bytes 3237892
  52.9 5.3 %collective-permute-start.1 = (f32[30,256]{1,0:T(8,128)S(1)}, f32[30,256]{1,0:T(8,128)S(1)}, u32[]{:S(2)}, u32[]{:S(2)}) collective-permute-start(f32[30,256]{1,0:T(8,128)S(1)} %slice.484), channel_id=1, source_target_pairs={{4,0},{8,4},{12,8},{16,12},{20,16},{24,20},{28,24},{5,1},{9,5},{13... | collective-permute-start | bytes 92168 | tf_op jit(solution)/shard_map/ppermute | solution.py:20
  59.0 2.8 %copy-start.2 = (bf16[1024,2048]{1,0:T(8,128)(2,1)S(1)}, bf16[1024,2048]{1,0:T(8,128)(2,1)}, u32[]{:S(2)}) copy-start(bf16[1024,2048]{1,0:T(8,128)(2,1)} %bi.1) | copy-start | bytes 12582916
  60.9 1.4 %copy-start.4 = (bf16[2048,256]{1,0:T(8,128)(2,1)S(1)}, bf16[2048,256]{1,0:T(8,128)(2,1)}, u32[]{:S(2)}) copy-start(bf16[2048,256]{1,0:T(8,128)(2,1)} %wv.1) | copy-start | bytes 3145732
  62.3 2.2 %copy-start.3 = (bf16[1024,2048]{1,0:T(8,128)(2,1)S(1)}, bf16[1024,2048]{1,0:T(8,128)(2,1)}, u32[]{:S(2)}) copy-start(bf16[1024,2048]{1,0:T(8,128)(2,1)} %og_hbm.1) | copy-start | bytes 12582916
